TPU v7x, 128 devices: a whole 4x4x4 slice. The times are simulated.
128 devices in a mesh: sp: 16 (over z, x), dp: 8 (over y, core).
Axes of the slice: x: 4, y: 4, z: 4, core: 2. Of those that a mesh axis runs over, the one named last changes fastest.
Arguments:
- residual_in: bfloat16 [8, 2048, 2048], P('dp', 'sp'), may hold values from -6 to 6
- query_rows: bfloat16 [8, 2048, 1024], P('dp', 'sp'), may hold values from -40 to 40
- key_rows: bfloat16 [8, 2048, 1024], P('dp', 'sp'), may hold values from -40 to 40
- value_rows: bfloat16 [8, 2048, 1024], P('dp', 'sp'), may hold values from -6 to 6
- gate_sums: float32 [8, 16, 2048], P('dp', 'sp'), as said below
- out_weight: bfloat16 [1024, 2048], replicated, may hold values from -0.1875 to 0.1875
- mix_gain: float32 [2048], replicated, may hold values from 0.1 to 1.9
- ffn_gain: float32 [2048], replicated, may hold values from 0.1 to 1.9
- expert_ids: int32 [8, 2048, 4], P('dp', 'sp'), may hold values from 0 to 127, all different within a row; in each aligned block of 128 rows (0 to 127, 128 to 255, ..., all dimensions but the last counted through in order) at most 8 rows name the same one
- route_weights: float32 [8, 2048, 4], P('dp', 'sp'), may hold values from 0.3 to 2
- expert_gate: bfloat16 [128, 2048, 512], P(('sp', 'dp')), may hold values from -0.125 to 0.125
- expert_up: bfloat16 [128, 2048, 512], P(('sp', 'dp')), may hold values from -0.125 to 0.125
- expert_down: bfloat16 [128, 512, 2048], P(('sp', 'dp')), may hold values from -0.25 to 0.25
- shared_gate: bfloat16 [2048, 512], replicated, may hold values from -0.125 to 0.125
- shared_up: bfloat16 [2048, 512], replicated, may hold values from -0.125 to 0.125
- shared_down: bfloat16 [512, 2048], replicated, may hold values from -0.25 to 0.25
Outputs:
- result_rows: bfloat16 [8, 2048, 2048], P('dp', 'sp')
Inputs may be any that keep to these rules, and one draw needn't show every extreme that they name: `expert_ids`: each row names 4 different experts. In the rows of one device no expert is named more than 8 times, a bound that some block reaches in some devices' rows. `gate_sums`: Non-increasing along positions for every sequence and head.
All inputs are finite; a program needn't handle non-finite values.
Results may differ from a plain program's by a relative error of at most 0.0071.
Values may be sent and summed in bfloat16 or wider, within the bound.
A program may use at most 128 MiB of HBM per device.

v0:
```python
import jax
import jax.numpy as jnp
from jax import lax
from jax.sharding import PartitionSpec as P

HEAD_DIM = 64


def sent_together(arrays, axis, split_dim, concat_dim, along):
    both = jnp.concatenate(arrays, axis=along)
    out, at, gathered = (
        lax.all_to_all(both, axis, split_axis=split_dim, concat_axis=concat_dim, tiled=True),
        0,
        [],
    )
    for a in arrays:
        gathered.append(lax.slice_in_dim(out, at, at + a.shape[along], axis=along))
        at += a.shape[along]
    return tuple(gathered)


def attend(query_all, key_all, value_all, gate_sums):
    length = query_all.shape[1]
    head_count = gate_sums.shape[1]
    score_scale = HEAD_DIM ** (-0.5)
    query_heads = query_all[0].reshape(length, head_count, HEAD_DIM)
    key_heads = key_all[0].reshape(length, head_count, HEAD_DIM)
    value_heads = value_all[0].reshape(length, head_count, HEAD_DIM)
    sums_local = gate_sums[0]
    block_rows = min(512, length)
    pieces = []
    for block_index in range(length // block_rows):
        start = block_index * block_rows
        block_end = start + block_rows
        scores = (
            jnp.einsum(
                "qhd,khd->hqk",
                query_heads[start:block_end],
                key_heads[:block_end],
                preferred_element_type=jnp.float32,
            )
            * score_scale
        )
        scores = scores + sums_local[:, start:block_end, None] - sums_local[:, None, :block_end]
        causal_mask = jnp.arange(block_end)[None, :] <= jnp.arange(start, block_end)[:, None]
        scores = jnp.where(causal_mask[None], scores, -jnp.inf)
        peak = jnp.max(scores, axis=2, keepdims=True)
        weights = jnp.exp(scores - peak)
        weights = (weights / jnp.sum(weights, axis=2, keepdims=True)).astype(jnp.bfloat16)
        mixed_heads = jnp.einsum(
            "hqk,khd->qhd", weights, value_heads[:block_end], preferred_element_type=jnp.float32
        ).astype(jnp.bfloat16)
        pieces.append(mixed_heads.reshape(block_rows, head_count * HEAD_DIM))
    return jnp.concatenate(pieces, axis=0)[None]


def gated_rows(rows_in, gate_w, up_w):
    gate_rows = jnp.dot(rows_in, gate_w, preferred_element_type=jnp.float32)
    up_rows = jnp.dot(rows_in, up_w, preferred_element_type=jnp.float32)
    return (jax.nn.silu(gate_rows) * up_rows).astype(jnp.bfloat16)


def shards(
    residual_in,
    query_rows,
    key_rows,
    value_rows,
    gate_sums,
    out_weight,
    mix_gain,
    ffn_gain,
    expert_ids,
    route_weights,
    expert_gate,
    expert_up,
    expert_down,
    shared_gate,
    shared_up,
    shared_down,
):
    key_all, value_all = sent_together((key_rows, value_rows), "sp", 2, 1, 0)
    query_all = lax.all_to_all(query_rows, "sp", split_axis=2, concat_axis=1, tiled=True)
    attended = attend(query_all, key_all, value_all, gate_sums)
    returned = lax.all_to_all(attended, "sp", split_axis=1, concat_axis=2, tiled=True)
    projected = jnp.dot(returned[0], out_weight, preferred_element_type=jnp.float32)
    residual_f = residual_in[0].astype(jnp.float32)
    mixed_rows = residual_f + mix_gain * projected * lax.rsqrt(
        jnp.mean(projected * projected, axis=1, keepdims=True) + 1e-06
    )
    normed = (
        ffn_gain
        * mixed_rows
        * lax.rsqrt(jnp.mean(mixed_rows * mixed_rows, axis=1, keepdims=True) + 1e-06)
    ).astype(jnp.bfloat16)
    shared_hidden = gated_rows(normed, shared_gate, shared_up)
    shared_out = jnp.dot(shared_hidden, shared_down, preferred_element_type=jnp.float32)
    tok_count = residual_in.shape[1]
    top_count = expert_ids.shape[2]
    width = residual_in.shape[2]
    sp_count = lax.axis_size("sp")
    dp_count = lax.axis_size("dp")
    expert_count = sp_count * dp_count
    capacity = 2 * tok_count * top_count // expert_count
    expert_list = expert_ids[0].reshape(tok_count * top_count)
    one_hot = (expert_list[:, None] == jnp.arange(expert_count, dtype=jnp.int32)[None, :]).astype(
        jnp.int32
    )
    position_in = jnp.sum((jnp.cumsum(one_hot, axis=0) - one_hot) * one_hot, axis=1)
    slot_index = expert_list * capacity + position_in
    repeated = jnp.repeat(normed, top_count, axis=0)
    outgoing = (
        jnp.zeros((expert_count * capacity, width), jnp.bfloat16).at[slot_index].set(repeated)
    )
    arrived = lax.all_to_all(
        outgoing.reshape(expert_count, capacity, width),
        ("sp", "dp"),
        split_axis=0,
        concat_axis=0,
        tiled=True,
    )
    flat_rows = arrived.reshape(-1, width)
    hidden = gated_rows(flat_rows, expert_gate[0], expert_up[0])
    finished = jnp.dot(hidden, expert_down[0], preferred_element_type=jnp.float32).astype(
        jnp.bfloat16
    )
    received = lax.all_to_all(
        finished.reshape(arrived.shape), ("sp", "dp"), split_axis=0, concat_axis=0, tiled=True
    )
    picked = received.reshape(expert_count * capacity, width)[slot_index]
    picked = picked.reshape(tok_count, top_count, width).astype(jnp.float32)
    routed = jnp.sum(picked * route_weights[0][:, :, None], axis=1)
    result_rows = (mixed_rows + shared_out + routed).astype(jnp.bfloat16)
    return result_rows[None]


def solution(mesh):
    return jax.shard_map(
        shards,
        mesh=mesh,
        in_specs=(
            P("dp", "sp", None),
            P("dp", "sp", None),
            P("dp", "sp", None),
            P("dp", "sp", None),
            P("dp", "sp", None),
            P(),
            P(),
            P(),
            P("dp", "sp", None),
            P("dp", "sp", None),
            P(("sp", "dp"), None, None),
            P(("sp", "dp"), None, None),
            P(("sp", "dp"), None, None),
            P(),
            P(),
            P(),
        ),
        out_specs=P("dp", "sp", None),
        check_vma=False,
    )
```

profile of v0, /device:TPU:1, one launch (start us, length us, event | category | flops | bytes accessed | tf_op | source)
XLA Modules:
  0.0 250.5 jit_solution(5828033538453089363)
XLA Ops:
  0.0 1.4 copy.68
  1.5 0.6 broadcast.177
  2.0 2.2 reduce.18
  4.2 0.8 reshape.330
  5.0 8.5 %all-to-all-start.1 = ((bf16[16,2,4096]{2,1,0:T(2,128)(2,1)}), bf16[16,2,4096]{2,1,0:T(2,128)(2,1)}, u32[]{:S(2)}, u32[]{:S(2)}) async-start(bf16[16,2,4096]{2,1,0:T(2,128)(2,1)} %reshape.330), calls=%async_computation.1 | async-start | bytes 524288 | tf_op jit(solution)/shard_map/all_to_all | solution.py:82
  13.5 0.6 iota_add_fusion.2
  14.1 0.1 copy.83
  14.2 0.6 broadcast_multiply_fusion
  14.8 0.4 copy.63
  15.2 0.4 copy.64
  15.6 0.1 eq.29
  15.7 0.1 copy.85
  15.8 0.2 fusion.48
  16.1 2.0 pad_maximum_fusion
  18.1 2.9 %all-to-all-done.1 = bf16[16,2,4096]{2,1,0:T(2,128)(2,1)} async-done(((bf16[16,2,4096]{2,1,0:T(2,128)(2,1)}), bf16[16,2,4096]{2,1,0:T(2,128)(2,1)}, u32[]{:S(2)}, u32[]{:S(2)}) %all-to-all-start.1) | async-done | bytes 262176 | tf_op jit(solution)/shard_map/all_to_all | solution.py:82
  21.1 4.0 %all-to-all-start = ((bf16[2,128,1024]{1,0,2:T(2,128)(2,1)}), bf16[2,128,1024]{1,0,2:T(2,128)(2,1)S(1)}, u32[]{:S(2)}, u32[]{:S(2)}) async-start(bf16[2,128,1024]{1,0,2:T(2,128)(2,1)} %pad_maximum_fusion), calls=%async_computation | async-start | bytes 1048576 | tf_op jit(solution)/shard_map/all_to_all | solution.py:12
  25.2 0.7 copy.86
  25.9 2.2 reshape.331
  28.4 6.5 %all-to-all-done = bf16[2,128,1024]{1,0,2:T(2,128)(2,1)S(1)} async-done(((bf16[2,128,1024]{1,0,2:T(2,128)(2,1)}), bf16[2,128,1024]{1,0,2:T(2,128)(2,1)S(1)}, u32[]{:S(2)}, u32[]{:S(2)}) %all-to-all-start) | async-done | bytes 524320 | tf_op jit(solution)/shard_map/all_to_all | solution.py:12
  35.3 0.1 copy.74
  35.4 0.1 copy.73
  35.7 0.2 copy.77
  35.9 0.2 copy.76
  36.1 0.7 fusion.87
  36.7 0.4 fusion.19
  37.1 0.5 fusion.34
  37.6 0.9 fusion.86
  38.5 0.5 fusion.9
  39.0 0.7 fusion.33
  39.7 0.3 fusion.88
  40.0 0.2 fusion.41
  40.2 0.3 fusion.35
  40.5 1.1 fusion.85
  41.7 0.6 fusion.4
  42.3 0.8 fusion.32
  43.2 0.7 copy.79
  43.9 12.7 %reduce.19 = bf16[2048,64]{1,0:T(8,128)(2,1)} reduce(bf16[2048,1,64]{2,1,0:T(2,128)(2,1)S(1)} %bitcast.230, bf16[]{:T(256)} %broadcast.177), dimensions={1}, to_apply=%bitcast.196.reduce_sub_computation | reduce | bytes 524290
  56.6 2.1 reshape.332
  58.7 4.1 %all-to-all-start.2 = ((bf16[16,2,4096]{2,1,0:T(2,128)(2,1)}), bf16[16,2,4096]{2,1,0:T(2,128)(2,1)S(1)}, u32[]{:S(2)}, u32[]{:S(2)}) async-start(bf16[16,2,4096]{2,1,0:T(2,128)(2,1)} %reshape.332), calls=%async_computation.2 | async-start | bytes 524288 | tf_op jit(solution)/shard_map/all_to_all | solution.py:84
  62.8 1.2 fusion.47
  64.0 0.1 copy.82
  64.1 0.1 mul.135
  64.2 6.2 %all-to-all-done.2 = bf16[16,2,4096]{2,1,0:T(2,128)(2,1)S(1)} async-done(((bf16[16,2,4096]{2,1,0:T(2,128)(2,1)}), bf16[16,2,4096]{2,1,0:T(2,128)(2,1)S(1)}, u32[]{:S(2)}, u32[]{:S(2)}) %all-to-all-start.2) | async-done | bytes 262176 | tf_op jit(solution)/shard_map/all_to_all | solution.py:84
  70.5 0.6 reshape.333
  71.1 0.6 copy.80
  71.9 3.1 %multiply_reduce_fusion.2 = (f32[128]{0:T(128)S(1)}, f32[128,2048]{1,0:T(8,128)S(1)}) fusion(bf16[128,1024]{0,1:T(8,128)(2,1)S(1)} %bitcast.235, bf16[1024,2048]{1,0:T(8,128)(2,1)} %param.21), kind=kOutput, calls=%fused_computation.58 | convolution fusion | flops 537395072 | bytes 5505536 | tf_op jit(solution)/shard_map/dot_general | solution.py:85
  74.9 0.3 multiply_reduce_fusion.1
  75.3 0.4 multiply_convert_fusion.1
  75.7 0.8 copy-done.1
  76.6 2.4 broadcast_in_dim.29
  79.0 4.0 %reshape.323 = bf16[512,2048]{1,0:T(8,128)(2,1)} reshape(bf16[128,4,2048]{2,1,0:T(4,128)(2,1)} %broadcast_in_dim.29) | data formatting | bytes 4194304 | tf_op jit(solution)/shard_map/reshape | solution.py:110
  82.9 7.2 %scatter_custom_fusion = bf16[1024,2048]{1,0:T(8,128)(2,1)} fusion(s32[512]{0:T(512)S(1)} %bitcast.257, bf16[512,2048]{1,0:T(8,128)(2,1)} %reshape.323, bf16[]{:T(256)} %constant.10.clone.1), kind=kCustom, calls=%fused_computation.31 | custom fusion | bytes 4194816 | tf_op jit(solution)/shard_map/scatter | solution.py:112
  90.1 62.2 %all_to_all.55 = bf16[128,8,2048]{2,1,0:T(8,128)(2,1)S(1)} all-to-all(bf16[128,8,2048]{2,1,0:T(8,128)(2,1)} %bitcast.224), channel_id=1, replica_groups=mesh['sp'=16,'dp'=8] {'sp','dp'}, dimensions={0} | all-to-all | bytes 8388608 | tf_op jit(solution)/shard_map/all_to_all | solution.py:114
  152.3 2.0 copy-done.3
  154.3 3.7 %fusion.2 = f32[1024,512]{1,0:T(8,128)} fusion(bf16[128,8,2048]{2,1,0:T(8,128)(2,1)S(1)} %all_to_all.55, bf16[1,2048,512]{2,1,0:T(8,128)(2,1)S(1)} %copy-done.13), kind=kOutput, calls=%fused_computation.4 | convolution fusion | flops 2147483648 | bytes 8388608 | tf_op jit(solution)/shard_map/dot_general | solution.py:58
  158.0 10.0 %convert_bitcast_fusion = bf16[128,8,2048]{2,1,0:T(8,128)(2,1)} fusion(bf16[1,512,2048]{2,1,0:T(8,128)(2,1)S(1)} %copy-done, f32[1024,512]{1,0:T(8,128)} %fusion.2, bf16[1,2048,512]{2,1,0:T(8,128)(2,1)} %param.27, bf16[128,8,2048]{2,1,0:T(8,128)(2,1)} %copy-done.3), kind=kOutput, calls=%fused_computation.8 | convolution fusion | flops 4300210176 | bytes 14680064 | tf_op jit(solution)/shard_map/dot_general | solution.py:123
  168.0 6.0 %all-to-all-start.4 = ((bf16[128,8,2048]{2,1,0:T(8,128)(2,1)}), bf16[128,8,2048]{2,1,0:T(8,128)(2,1)}, u32[]{:S(2)}, u32[]{:S(2)}) async-start(bf16[128,8,2048]{2,1,0:T(8,128)(2,1)} %convert_bitcast_fusion), calls=%async_computation.4 | async-start | bytes 8388608 | tf_op jit(solution)/shard_map/all_to_all | solution.py:126
  174.0 0.1 copy.87
  174.1 2.2 fusion.89
  176.4 50.3 %all-to-all-done.4 = bf16[128,8,2048]{2,1,0:T(8,128)(2,1)} async-done(((bf16[128,8,2048]{2,1,0:T(8,128)(2,1)}), bf16[128,8,2048]{2,1,0:T(8,128)(2,1)}, u32[]{:S(2)}, u32[]{:S(2)}) %all-to-all-start.4) | async-done | bytes 4194336 | tf_op jit(solution)/shard_map/all_to_all | solution.py:126
  226.7 8.0 %gather_fusion = bf16[512,2048]{1,0:T(8,128)(2,1)} fusion(bf16[1024,2048]{1,0:T(8,128)(2,1)} %bitcast.42, s32[1024]{0:T(1024)S(1)} %pad_clamp_fusion), kind=kCustom, calls=%fused_computation | custom fusion | bytes 4196352 | tf_op jit(solution)/shard_map/gather | solution.py:129
  234.7 4.8 %reshape.310 = f32[128,4,2048]{2,1,0:T(4,128)} reshape(bf16[512,2048]{1,0:T(8,128)(2,1)} %gather_fusion) | data formatting | bytes 6291456 | tf_op jit(solution)/shard_map/convert_element_type | solution.py:130
  239.4 6.3 %multiply_reduce_fusion = f32[128,2048]{1,0:T(8,128)} fusion(f32[128,4,2048]{2,1,0:T(4,128)} %reshape.310, f32[128,4]{1,0:T(8,128)S(1)} %copy.87), kind=kLoop, calls=%fused_computation.7 | loop fusion | flops 1835008 | bytes 5244928 | tf_op jit(solution)/shard_map/reduce_sum | solution.py:131
  245.7 4.5 %fusion.12 = bf16[1,128,2048]{2,1,0:T(8,128)(2,1)} fusion(f32[128,2048]{1,0:T(8,128)} %multiply_reduce_fusion, bf16[512,2048]{1,0:T(8,128)(2,1)} %param.31, bf16[128,2048]{1,0:T(8,128)(2,1)} %copy-done.1, bf16[2048,512]{1,0:T(8,128)(2,1)} %param.30, f32[128,512]{1,0:T(8,128)S(1)} %fusion.89, f32[128]{0:T(128)S(1)} %add_rsqrt_fusion.1, ...), kind=kOutput, calls=%fused_computation.25 | convolution fusion | flops 539099136 | bytes 8135168 | tf_op jit(solution)/shard_map/dot_general | solution.py:96
  (59 shorter events, 1.2 us)
Async XLA Ops:
  0.0 158.0 %copy-start = (bf16[1,512,2048]{2,1,0:T(8,128)(2,1)S(1)}, bf16[1,512,2048]{2,1,0:T(8,128)(2,1)}, u32[]{:S(2)}) copy-start(bf16[1,512,2048]{2,1,0:T(8,128)(2,1)} %param.28) | copy-start | bytes 6291460
  0.0 14.1 %copy-start.9 = (s32[1,128,4]{1,2,0:T(4,128)S(1)}, s32[1,128,4]{1,2,0:T(4,128)}, u32[]{:S(2)}) copy-start(s32[1,128,4]{1,2,0:T(4,128)} %param.24) | copy-start | bytes 6148
  0.0 14.8 %copy-start.4 = (bf16[1,128,1024]{2,1,0:T(8,128)(2,1)S(1)}, bf16[1,128,1024]{2,1,0:T(8,128)(2,1)}, u32[]{:S(2)}) copy-start(bf16[1,128,1024]{2,1,0:T(8,128)(2,1)} %param.18) | copy-start | bytes 786436
  0.0 15.2 %copy-start.5 = (bf16[1,128,1024]{2,1,0:T(8,128)(2,1)S(1)}, bf16[1,128,1024]{2,1,0:T(8,128)(2,1)}, u32[]{:S(2)}) copy-start(bf16[1,128,1024]{2,1,0:T(8,128)(2,1)} %param.19) | copy-start | bytes 786436
  0.0 15.6 %copy-start.7 = (f32[1,1,2048]{2,1,0:T(1,128)S(1)}, f32[1,1,2048]{2,1,0:T(1,128)}, u32[]{:S(2)}) copy-start(f32[1,1,2048]{2,1,0:T(1,128)} %param.20) | copy-start | bytes 24580
  5.0 16.1 %all-to-all-start.1 = ((bf16[16,2,4096]{2,1,0:T(2,128)(2,1)}), bf16[16,2,4096]{2,1,0:T(2,128)(2,1)}, u32[]{:S(2)}, u32[]{:S(2)}) async-start(bf16[16,2,4096]{2,1,0:T(2,128)(2,1)} %reshape.330), calls=%async_computation.1 | async-start | bytes 524288 | tf_op jit(solution)/shard_map/all_to_all | solution.py:82
  21.1 13.8 %all-to-all-start = ((bf16[2,128,1024]{1,0,2:T(2,128)(2,1)}), bf16[2,128,1024]{1,0,2:T(2,128)(2,1)S(1)}, u32[]{:S(2)}, u32[]{:S(2)}) async-start(bf16[2,128,1024]{1,0,2:T(2,128)(2,1)} %pad_maximum_fusion), calls=%async_computation | async-start | bytes 1048576 | tf_op jit(solution)/shard_map/all_to_all | solution.py:12
  35.0 1.0 copy-start.12
  43.1 20.8 %copy-start.10 = (s32[1,128,4]{1,2,0:T(4,128)S(1)}, s32[1,128,4]{1,2,0:T(4,128)}, u32[]{:S(2)}) copy-start(s32[1,128,4]{1,2,0:T(4,128)} %broadcast_multiply_fusion) | copy-start | bytes 6148
  58.7 11.8 %all-to-all-start.2 = ((bf16[16,2,4096]{2,1,0:T(2,128)(2,1)}), bf16[16,2,4096]{2,1,0:T(2,128)(2,1)S(1)}, u32[]{:S(2)}, u32[]{:S(2)}) async-start(bf16[16,2,4096]{2,1,0:T(2,128)(2,1)} %reshape.332), calls=%async_computation.2 | async-start | bytes 524288 | tf_op jit(solution)/shard_map/all_to_all | solution.py:84
  71.8 3.1 %copy-start.2 = (bf16[1,128,2048]{2,1,0:T(8,128)(2,1)S(1)}, bf16[1,128,2048]{2,1,0:T(8,128)(2,1)}, u32[]{:S(2)}) copy-start(bf16[1,128,2048]{2,1,0:T(8,128)(2,1)} %param.16) | copy-start | bytes 1572868
  71.8 3.1 %copy-start.6 = (f32[2048]{0:T(1024)S(1)}, f32[2048]{0:T(1024)}, u32[]{:S(2)}) copy-start(f32[2048]{0:T(1024)} %param.22) | copy-start | bytes 24580
  71.8 3.5 %copy-start.8 = (f32[2048]{0:T(1024)S(1)}, f32[2048]{0:T(1024)}, u32[]{:S(2)}) copy-start(f32[2048]{0:T(1024)} %param.23) | copy-start | bytes 24580
  75.7 0.8 copy-start.1
  90.1 64.2 %copy-start.13 = (bf16[1,2048,512]{2,1,0:T(8,128)(2,1)S(1)}, bf16[1,2048,512]{2,1,0:T(8,128)(2,1)}, u32[]{:S(2)}) copy-start(bf16[1,2048,512]{2,1,0:T(8,128)(2,1)} %param.26) | copy-start | bytes 6291460
  152.3 2.0 copy-start.3
  168.0 6.0 %copy-start.11 = (f32[1,128,4]{1,2,0:T(4,128)S(1)}, f32[1,128,4]{1,2,0:T(4,128)}, u32[]{:S(2)}) copy-start(f32[1,128,4]{1,2,0:T(4,128)} %param.25) | copy-start | bytes 6148
  168.0 58.7 %all-to-all-start.4 = ((bf16[128,8,2048]{2,1,0:T(8,128)(2,1)}), bf16[128,8,2048]{2,1,0:T(8,128)(2,1)}, u32[]{:S(2)}, u32[]{:S(2)}) async-start(bf16[128,8,2048]{2,1,0:T(8,128)(2,1)} %convert_bitcast_fusion), calls=%async_computation.4 | async-start | bytes 8388608 | tf_op jit(solution)/shard_map/all_to_all | solution.py:126
where the time goes:
time: 255 us; the launch traced here: 251 us
  waiting for transfers between devices  66 us (26%)
  blocking collectives  62.2 us (24%)
  local copies, waits for them, and re-layouts  41.9 us (16%)
  matrix products  28.8 us (11%)
  other arithmetic  28.3 us (11%)
  starting transfers between devices  22.6 us (9%)
    all_to_all x1, blocking collectives, shards(): lax.all_to_all(outgoing.reshape(expert_count, capacity, width), ('sp', 'd...  62.2 us
    all_to_all x1, waiting for transfers between devices, shards(): lax.all_to_all(finished.reshape(arrived.shape), ('sp', 'dp'), split_axis=...  50.3 us
    unnamed x2, other arithmetic  14.9 us
    unnamed x40, local copies, waits for them, and re-layouts  11.5 us
    dot_general x1, matrix products, shards(): jnp.dot(hidden, expert_down[0], preferred_element_type=jnp.float32)  9.96 us
    all_to_all x1, starting transfers between devices, shards(): lax.all_to_all(query_rows, 'sp', split_axis=2, concat_axis=1, tiled=True)  8.47 us
    gather x1, local copies, waits for them, and re-layouts, shards(): picked = received.reshape(expert_count * capacity, width)[slot_index]  7.96 us
    scatter x1, local copies, waits for them, and re-layouts, shards(): jnp.zeros((expert_count * capacity, width), jnp.bfloat16).at[slot_index]  7.21 us
  transfers between devices with their start and end apart: 4, of which 4 were waited for; matrix products, arithmetic and copies ran while one was open for 5% of the time, Pallas kernels for 0%

commit v1 on v0

--- a/solution.py
+++ b/solution.py
@@ -81,7 +81,10 @@
     key_all, value_all = sent_together((key_rows, value_rows), "sp", 2, 1, 0)
     query_all = lax.all_to_all(query_rows, "sp", split_axis=2, concat_axis=1, tiled=True)
     attended = attend(query_all, key_all, value_all, gate_sums)
-    returned = lax.all_to_all(attended, "sp", split_axis=1, concat_axis=2, tiled=True)
+    returned = jnp.concatenate(
+        lax.all_to_all(jnp.stack(jnp.split(attended, lax.axis_size("sp"), axis=1)), "sp", 0, 0),
+        axis=2,
+    )
     projected = jnp.dot(returned[0], out_weight, preferred_element_type=jnp.float32)
     residual_f = residual_in[0].astype(jnp.float32)
     mixed_rows = residual_f + mix_gain * projected * lax.rsqrt(

time: 255 us -> 243 us (0.953); the launches traced: 251 us -> 242 us
  other arithmetic: 28.3 us -> 14.7 us
  local copies, waits for them, and re-layouts: 41.9 us -> 47.4 us
    unnamed x2 -> x1, other arithmetic: 14.9 us -> 2.21 us
    unnamed x40 -> x54, local copies, waits for them, and re-layouts: 11.5 us -> 17.8 us
  transfers between devices with their start and end apart: 4 -> 4, of which waited for: 4 -> 4; matrix products, arithmetic and copies ran while one was open for 5% -> 4% of each run, Pallas kernels for 0% -> 0%
where the time goes in v1:
time: 243 us; the launch traced here: 242 us
  waiting for transfers between devices  66.8 us (27%)
  blocking collectives  62 us (26%)
  local copies, waits for them, and re-layouts  47.4 us (20%)
  matrix products  28.8 us (12%)
  starting transfers between devices  21.6 us (9%)
  other arithmetic  14.7 us (6%)
    all_to_all x1, blocking collectives, shards(): lax.all_to_all(outgoing.reshape(expert_count, capacity, width), ('sp', 'd...  62 us
    all_to_all x1, waiting for transfers between devices, shards(): lax.all_to_all(finished.reshape(arrived.shape), ('sp', 'dp'), split_axis=...  50.5 us
    unnamed x54, local copies, waits for them, and re-layouts  17.8 us
    dot_general x1, matrix products, shards(): jnp.dot(hidden, expert_down[0], preferred_element_type=jnp.float32)  9.96 us
    all_to_all x1, starting transfers between devices, shards(): lax.all_to_all(query_rows, 'sp', split_axis=2, concat_axis=1, tiled=True)  8.47 us
    gather x1, local copies, waits for them, and re-layouts, shards(): picked = received.reshape(expert_count * capacity, width)[slot_index]  7.96 us
    scatter x1, local copies, waits for them, and re-layouts, shards(): jnp.zeros((expert_count * capacity, width), jnp.bfloat16).at[slot_index]  7.21 us
    all_to_all x1, waiting for transfers between devices, shards(): lax.all_to_all(jnp.stack(jnp.split(attended, lax.axis_size('sp'), axis=1)...  6.92 us
  transfers between devices with their start and end apart: 4, of which 4 were waited for; matrix products, arithmetic and copies ran while one was open for 4% of the time, Pallas kernels for 0%

profile of v1, /device:TPU:1, one launch (start us, length us, event | category | flops | bytes accessed | tf_op | source)
XLA Modules:
  0.0 241.8 jit_solution(14440088158304944297)
XLA Ops:
  0.0 1.4 copy.44
  1.5 0.5 broadcast.177
  2.0 2.2 reduce.18
  4.2 0.8 reshape.333
  4.9 8.5 %all-to-all-start.1 = ((bf16[16,2,4096]{2,1,0:T(2,128)(2,1)}), bf16[16,2,4096]{2,1,0:T(2,128)(2,1)}, u32[]{:S(2)}, u32[]{:S(2)}) async-start(bf16[16,2,4096]{2,1,0:T(2,128)(2,1)} %reshape.333), calls=%async_computation.1 | async-start | bytes 524288 | tf_op jit(solution)/shard_map/all_to_all | solution.py:82
  13.4 0.6 iota_add_fusion.2
  14.1 0.6 broadcast_multiply_fusion
  14.7 0.4 copy.39
  15.1 0.4 copy.40
  15.8 0.2 fusion.48
  16.0 2.0 pad_maximum_fusion
  18.1 2.9 %all-to-all-done.1 = bf16[16,2,4096]{2,1,0:T(2,128)(2,1)} async-done(((bf16[16,2,4096]{2,1,0:T(2,128)(2,1)}), bf16[16,2,4096]{2,1,0:T(2,128)(2,1)}, u32[]{:S(2)}, u32[]{:S(2)}) %all-to-all-start.1) | async-done | bytes 262176 | tf_op jit(solution)/shard_map/all_to_all | solution.py:82
  21.0 3.8 %all-to-all-start = ((bf16[2,128,1024]{1,0,2:T(2,128)(2,1)}), bf16[2,128,1024]{1,0,2:T(2,128)(2,1)S(1)}, u32[]{:S(2)}, u32[]{:S(2)}) async-start(bf16[2,128,1024]{1,0,2:T(2,128)(2,1)} %pad_maximum_fusion), calls=%async_computation | async-start | bytes 1048576 | tf_op jit(solution)/shard_map/all_to_all | solution.py:12
  24.9 0.7 copy.59
  25.7 2.2 reshape.334
  28.1 6.4 %all-to-all-done = bf16[2,128,1024]{1,0,2:T(2,128)(2,1)S(1)} async-done(((bf16[2,128,1024]{1,0,2:T(2,128)(2,1)}), bf16[2,128,1024]{1,0,2:T(2,128)(2,1)S(1)}, u32[]{:S(2)}, u32[]{:S(2)}) %all-to-all-start) | async-done | bytes 524320 | tf_op jit(solution)/shard_map/all_to_all | solution.py:12
  35.7 0.7 fusion.87
  36.4 0.4 fusion.19
  36.8 0.5 fusion.34
  37.3 0.9 fusion.86
  38.2 0.5 fusion.9
  38.7 0.7 fusion.33
  39.3 0.3 fusion.88
  39.9 0.3 fusion.35
  40.2 1.1 fusion.85
  41.3 0.6 fusion.4
  42.0 0.8 fusion.32
  42.8 0.6 constant_dynamic-update-slice_fusion.15
  43.4 0.6 constant_dynamic-update-slice_fusion.14
  44.0 0.6 constant_dynamic-update-slice_fusion.13
  44.7 0.6 constant_dynamic-update-slice_fusion.12
  45.3 0.6 constant_dynamic-update-slice_fusion.11
  45.9 0.6 constant_dynamic-update-slice_fusion.10
  46.5 0.6 constant_dynamic-update-slice_fusion.9
  47.1 0.6 constant_dynamic-update-slice_fusion.8
  47.7 0.6 constant_dynamic-update-slice_fusion.7
  48.3 0.6 constant_dynamic-update-slice_fusion.6
  48.9 0.6 constant_dynamic-update-slice_fusion.5
  49.5 0.6 constant_dynamic-update-slice_fusion.4
  50.2 0.6 constant_dynamic-update-slice_fusion.3
  50.8 0.6 constant_dynamic-update-slice_fusion.2
  51.4 0.6 constant_dynamic-update-slice_fusion.1
  52.0 0.6 constant_dynamic-update-slice_fusion
  52.6 3.8 %all-to-all-start.2 = ((bf16[16,1,128,64]{2,3,1,0:T(8,128)(2,1)}), bf16[16,1,128,64]{2,3,1,0:T(8,128)(2,1)S(1)}, u32[]{:S(2)}, u32[]{:S(2)}) async-start(bf16[16,1,128,64]{2,3,1,0:T(8,128)(2,1)} %constant_dynamic-update-slice_fusion), calls=%async_computation.2 | async-start | bytes 524288 | tf_op jit(solution)/shard_map/all_to_all | solution.py:85
  56.4 0.2 fusion.47
  56.9 6.9 %all-to-all-done.2 = bf16[16,1,128,64]{2,3,1,0:T(8,128)(2,1)S(1)} async-done(((bf16[16,1,128,64]{2,3,1,0:T(8,128)(2,1)}), bf16[16,1,128,64]{2,3,1,0:T(8,128)(2,1)S(1)}, u32[]{:S(2)}, u32[]{:S(2)}) %all-to-all-start.2) | async-done | bytes 262176 | tf_op jit(solution)/shard_map/all_to_all | solution.py:85
  63.8 3.1 %multiply_reduce_fusion.2 = (f32[128]{0:T(128)S(1)}, f32[128,2048]{1,0:T(8,128)S(1)}) fusion(bf16[128,1024]{0,1:T(8,128)(2,1)S(1)} %bitcast.288, bf16[1024,2048]{1,0:T(8,128)(2,1)} %param.21), kind=kOutput, calls=%fused_computation.58 | convolution fusion | flops 537395072 | bytes 5505536 | tf_op jit(solution)/shard_map/dot_general | solution.py:88
  66.9 0.3 multiply_reduce_fusion.1
  67.2 0.4 multiply_convert_fusion.1
  67.7 0.8 copy-done.1
  68.5 2.4 broadcast_in_dim.29
  70.9 4.0 %reshape.326 = bf16[512,2048]{1,0:T(8,128)(2,1)} reshape(bf16[128,4,2048]{2,1,0:T(4,128)(2,1)} %broadcast_in_dim.29) | data formatting | bytes 4194304 | tf_op jit(solution)/shard_map/reshape | solution.py:113
  74.9 7.2 %scatter_custom_fusion = bf16[1024,2048]{1,0:T(8,128)(2,1)} fusion(s32[512]{0:T(512)S(1)} %bitcast.309, bf16[512,2048]{1,0:T(8,128)(2,1)} %reshape.326, bf16[]{:T(256)} %constant.10.clone.1), kind=kCustom, calls=%fused_computation.31 | custom fusion | bytes 4194816 | tf_op jit(solution)/shard_map/scatter | solution.py:115
  82.1 62.0 %all_to_all.45 = bf16[128,8,2048]{2,1,0:T(8,128)(2,1)S(1)} all-to-all(bf16[128,8,2048]{2,1,0:T(8,128)(2,1)} %bitcast.280), channel_id=1, replica_groups=mesh['sp'=16,'dp'=8] {'sp','dp'}, dimensions={0} | all-to-all | bytes 8388608 | tf_op jit(solution)/shard_map/all_to_all | solution.py:117
  144.1 2.0 copy-done.3
  146.1 3.7 %fusion.2 = f32[1024,512]{1,0:T(8,128)} fusion(bf16[128,8,2048]{2,1,0:T(8,128)(2,1)S(1)} %all_to_all.45, bf16[1,2048,512]{2,1,0:T(8,128)(2,1)S(1)} %copy-done.14), kind=kOutput, calls=%fused_computation.4 | convolution fusion | flops 2147483648 | bytes 8388608 | tf_op jit(solution)/shard_map/dot_general | solution.py:58
  149.8 10.0 %convert_bitcast_fusion = bf16[128,8,2048]{2,1,0:T(8,128)(2,1)} fusion(bf16[1,512,2048]{2,1,0:T(8,128)(2,1)S(1)} %copy-done, f32[1024,512]{1,0:T(8,128)} %fusion.2, bf16[1,2048,512]{2,1,0:T(8,128)(2,1)} %param.27, bf16[128,8,2048]{2,1,0:T(8,128)(2,1)} %copy-done.3), kind=kOutput, calls=%fused_computation.8 | convolution fusion | flops 4300210176 | bytes 14680064 | tf_op jit(solution)/shard_map/dot_general | solution.py:126
  159.7 5.6 %all-to-all-start.4 = ((bf16[128,8,2048]{2,1,0:T(8,128)(2,1)}), bf16[128,8,2048]{2,1,0:T(8,128)(2,1)}, u32[]{:S(2)}, u32[]{:S(2)}) async-start(bf16[128,8,2048]{2,1,0:T(8,128)(2,1)} %convert_bitcast_fusion), calls=%async_computation.4 | async-start | bytes 8388608 | tf_op jit(solution)/shard_map/all_to_all | solution.py:129
  165.5 2.2 fusion.89
  167.7 50.5 %all-to-all-done.4 = bf16[128,8,2048]{2,1,0:T(8,128)(2,1)} async-done(((bf16[128,8,2048]{2,1,0:T(8,128)(2,1)}), bf16[128,8,2048]{2,1,0:T(8,128)(2,1)}, u32[]{:S(2)}, u32[]{:S(2)}) %all-to-all-start.4) | async-done | bytes 4194336 | tf_op jit(solution)/shard_map/all_to_all | solution.py:129
  218.2 8.0 %gather_fusion = bf16[512,2048]{1,0:T(8,128)(2,1)} fusion(bf16[1024,2048]{1,0:T(8,128)(2,1)} %bitcast.58, s32[1024]{0:T(1024)S(1)} %pad_clamp_fusion), kind=kCustom, calls=%fused_computation | custom fusion | bytes 4196352 | tf_op jit(solution)/shard_map/gather | solution.py:132
  226.2 4.8 %reshape.313 = f32[128,4,2048]{2,1,0:T(4,128)} reshape(bf16[512,2048]{1,0:T(8,128)(2,1)} %gather_fusion) | data formatting | bytes 6291456 | tf_op jit(solution)/shard_map/convert_element_type | solution.py:133
  230.9 6.3 %multiply_reduce_fusion = f32[128,2048]{1,0:T(8,128)} fusion(f32[128,4,2048]{2,1,0:T(4,128)} %reshape.313, f32[128,4]{1,0:T(8,128)S(1)} %copy.60), kind=kLoop, calls=%fused_computation.7 | loop fusion | flops 1835008 | bytes 5244928 | tf_op jit(solution)/shard_map/reduce_sum | solution.py:134
  237.3 4.5 %fusion.12 = bf16[1,128,2048]{2,1,0:T(8,128)(2,1)} fusion(f32[128,2048]{1,0:T(8,128)} %multiply_reduce_fusion, bf16[512,2048]{1,0:T(8,128)(2,1)} %param.31, bf16[128,2048]{1,0:T(8,128)(2,1)} %copy-done.1, bf16[2048,512]{1,0:T(8,128)(2,1)} %param.30, f32[128,512]{1,0:T(8,128)S(1)} %fusion.89, f32[128]{0:T(128)S(1)} %add_rsqrt_fusion.1, ...), kind=kOutput, calls=%fused_computation.25 | convolution fusion | flops 539099136 | bytes 8135168 | tf_op jit(solution)/shard_map/dot_general | solution.py:99
  (70 shorter events, 2.5 us)
Async XLA Ops:
  0.0 149.8 %copy-start = (bf16[1,512,2048]{2,1,0:T(8,128)(2,1)S(1)}, bf16[1,512,2048]{2,1,0:T(8,128)(2,1)}, u32[]{:S(2)}) copy-start(bf16[1,512,2048]{2,1,0:T(8,128)(2,1)} %param.28) | copy-start | bytes 6291460
  0.0 14.0 %copy-start.10 = (s32[1,128,4]{1,2,0:T(4,128)S(1)}, s32[1,128,4]{1,2,0:T(4,128)}, u32[]{:S(2)}) copy-start(s32[1,128,4]{1,2,0:T(4,128)} %param.24) | copy-start | bytes 6148
  0.0 14.7 %copy-start.5 = (bf16[1,128,1024]{2,1,0:T(8,128)(2,1)S(1)}, bf16[1,128,1024]{2,1,0:T(8,128)(2,1)}, u32[]{:S(2)}) copy-start(bf16[1,128,1024]{2,1,0:T(8,128)(2,1)} %param.18) | copy-start | bytes 786436
  0.0 15.1 %copy-start.6 = (bf16[1,128,1024]{2,1,0:T(8,128)(2,1)S(1)}, bf16[1,128,1024]{2,1,0:T(8,128)(2,1)}, u32[]{:S(2)}) copy-start(bf16[1,128,1024]{2,1,0:T(8,128)(2,1)} %param.19) | copy-start | bytes 786436
  0.0 15.5 %copy-start.8 = (f32[1,1,2048]{2,1,0:T(1,128)S(1)}, f32[1,1,2048]{2,1,0:T(1,128)}, u32[]{:S(2)}) copy-start(f32[1,1,2048]{2,1,0:T(1,128)} %param.20) | copy-start | bytes 24580
  4.9 16.1 %all-to-all-start.1 = ((bf16[16,2,4096]{2,1,0:T(2,128)(2,1)}), bf16[16,2,4096]{2,1,0:T(2,128)(2,1)}, u32[]{:S(2)}, u32[]{:S(2)}) async-start(bf16[16,2,4096]{2,1,0:T(2,128)(2,1)} %reshape.333), calls=%async_computation.1 | async-start | bytes 524288 | tf_op jit(solution)/shard_map/all_to_all | solution.py:82
  21.0 13.5 %all-to-all-start = ((bf16[2,128,1024]{1,0,2:T(2,128)(2,1)}), bf16[2,128,1024]{1,0,2:T(2,128)(2,1)S(1)}, u32[]{:S(2)}, u32[]{:S(2)}) async-start(bf16[2,128,1024]{1,0,2:T(2,128)(2,1)} %pad_maximum_fusion), calls=%async_computation | async-start | bytes 1048576 | tf_op jit(solution)/shard_map/all_to_all | solution.py:12
  34.7 1.0 copy-start.13
  42.0 14.4 %copy-start.4 = (s32[128,4,128]{0,2,1:T(8,128)S(1)}, s32[128,4,128]{0,2,1:T(8,128)}, u32[]{:S(2)}) copy-start(s32[128,4,128]{0,2,1:T(8,128)} %copy.59) | copy-start | bytes 786436
  42.0 14.6 %copy-start.11 = (s32[1,128,4]{1,2,0:T(4,128)S(1)}, s32[1,128,4]{1,2,0:T(4,128)}, u32[]{:S(2)}) copy-start(s32[1,128,4]{1,2,0:T(4,128)} %broadcast_multiply_fusion) | copy-start | bytes 6148
  52.6 11.2 %all-to-all-start.2 = ((bf16[16,1,128,64]{2,3,1,0:T(8,128)(2,1)}), bf16[16,1,128,64]{2,3,1,0:T(8,128)(2,1)S(1)}, u32[]{:S(2)}, u32[]{:S(2)}) async-start(bf16[16,1,128,64]{2,3,1,0:T(8,128)(2,1)} %constant_dynamic-update-slice_fusion), calls=%async_computation.2 | async-start | bytes 524288 | tf_op jit(solution)/shard_map/all_to_all | solution.py:85
  63.8 3.1 %copy-start.2 = (bf16[1,128,2048]{2,1,0:T(8,128)(2,1)S(1)}, bf16[1,128,2048]{2,1,0:T(8,128)(2,1)}, u32[]{:S(2)}) copy-start(bf16[1,128,2048]{2,1,0:T(8,128)(2,1)} %param.16) | copy-start | bytes 1572868
  63.8 3.1 %copy-start.7 = (f32[2048]{0:T(1024)S(1)}, f32[2048]{0:T(1024)}, u32[]{:S(2)}) copy-start(f32[2048]{0:T(1024)} %param.22) | copy-start | bytes 24580
  63.8 3.5 %copy-start.9 = (f32[2048]{0:T(1024)S(1)}, f32[2048]{0:T(1024)}, u32[]{:S(2)}) copy-start(f32[2048]{0:T(1024)} %param.23) | copy-start | bytes 24580
  67.7 0.8 copy-start.1
  82.1 64.0 %copy-start.14 = (bf16[1,2048,512]{2,1,0:T(8,128)(2,1)S(1)}, bf16[1,2048,512]{2,1,0:T(8,128)(2,1)}, u32[]{:S(2)}) copy-start(bf16[1,2048,512]{2,1,0:T(8,128)(2,1)} %param.26) | copy-start | bytes 6291460
  144.1 2.0 copy-start.3
  159.7 5.6 %copy-start.12 = (f32[1,128,4]{1,2,0:T(4,128)S(1)}, f32[1,128,4]{1,2,0:T(4,128)}, u32[]{:S(2)}) copy-start(f32[1,128,4]{1,2,0:T(4,128)} %param.25) | copy-start | bytes 6148
  159.7 58.5 %all-to-all-start.4 = ((bf16[128,8,2048]{2,1,0:T(8,128)(2,1)}), bf16[128,8,2048]{2,1,0:T(8,128)(2,1)}, u32[]{:S(2)}, u32[]{:S(2)}) async-start(bf16[128,8,2048]{2,1,0:T(8,128)(2,1)} %convert_bitcast_fusion), calls=%async_computation.4 | async-start | bytes 8388608 | tf_op jit(solution)/shard_map/all_to_all | solution.py:129
